TPU v7x, 32 devices: a whole 2x2x4 slice. The times are simulated.
32 devices in a mesh: sp: 4 (over y, x), tp: 8 (over z, core).
Axes of the slice: x: 2, y: 2, z: 4, core: 2. Of those that a mesh axis runs over, the one named last changes fastest.
Arguments:
- target: bfloat16 [512, 2048], P('sp'), may hold values from -6 to 6
- source: bfloat16 [1536, 2048], P('sp'), may hold values from -6 to 6
- cotangent: bfloat16 [512, 2048], P('sp'), may hold values from -192 to 192
- target_gain: float32 [2048], replicated, may hold values from 0.1 to 1.9
- source_gain: float32 [2048], replicated, may hold values from 0.1 to 1.9
- w_query: bfloat16 [2048, 4096], P(None, 'tp'), may hold values from -0.125 to 0.125
- w_key: bfloat16 [2048, 128], replicated, may hold values from -0.125 to 0.125
- w_value: bfloat16 [2048, 128], replicated, may hold values from -0.125 to 0.125
- w_out: bfloat16 [4096, 2048], P('tp'), may hold values from -0.09375 to 0.09375
Outputs:
- grad_target: bfloat16 [512, 2048], P(('sp', 'tp'))
- grad_source: bfloat16 [1536, 2048], P(('sp', 'tp'))
- grad_out_w: bfloat16 [4096, 2048], P('tp', 'sp')
All inputs are finite; a program needn't handle non-finite values.
Results may differ from a plain program's by a relative error of at most 0.025.
Values may be sent and summed in bfloat16 or wider, within the bound.
A program may use at most 64 MiB of HBM per device.

v0:
```python
import jax
import jax.numpy as jnp
from jax import lax
from jax.sharding import PartitionSpec as P

HEAD = 128
NORM_EPS = 1e-06
KEY_BLOCK = 1024
QUERY_BLOCK = 256


def normed(row_block, gain_vec):
    rows_wide = row_block.astype(jnp.float32)
    inv_rms = lax.rsqrt(jnp.mean(rows_wide * rows_wide, axis=1, keepdims=True) + NORM_EPS)
    return (rows_wide * inv_rms * gain_vec).astype(jnp.bfloat16)


def norm_back(row_block, gain_vec, upstream):
    rows_wide = row_block.astype(jnp.float32)
    inv_rms = lax.rsqrt(jnp.mean(rows_wide * rows_wide, axis=1, keepdims=True) + NORM_EPS)
    unit_rows = rows_wide * inv_rms
    pulled = upstream * gain_vec
    return inv_rms * (pulled - unit_rows * jnp.mean(pulled * unit_rows, axis=1, keepdims=True))


def block_span(row_count, largest):
    if row_count > largest and row_count % largest == 0:
        return largest
    return row_count


def right_product(left_rows, weight_mat):
    return lax.dot_general(
        left_rows, weight_mat, (((1,), (1,)), ((), ())), preferred_element_type=jnp.float32
    )


def on_device(target, source, cotangent, target_gain, source_gain, w_query, w_key, w_value, w_out):
    tp_count = lax.axis_size("tp")
    tp_place = lax.axis_index("tp")
    group_rows = target.shape[0]
    q_width = w_query.shape[1]
    heads_here = q_width // HEAD
    inv_root = HEAD ** (-0.5)
    query_all = jnp.dot(
        normed(target, target_gain), w_query, preferred_element_type=jnp.float32
    ).astype(jnp.bfloat16)
    grad_all = right_product(cotangent, w_out).astype(jnp.bfloat16)
    cot_columns = lax.all_to_all(cotangent, "sp", split_axis=1, concat_axis=0, tiled=True)
    source_rows = source.shape[0] // tp_count
    source_part = lax.dynamic_slice_in_dim(source, tp_place * source_rows, source_rows, 0)
    source_normed = normed(source_part, source_gain)
    key_own = jnp.dot(source_normed, w_key, preferred_element_type=jnp.float32).astype(jnp.bfloat16)
    value_own = jnp.dot(source_normed, w_value, preferred_element_type=jnp.float32).astype(
        jnp.bfloat16
    )
    key_group, value_group = (
        lax.all_gather(key_own, "tp", axis=0, tiled=True),
        lax.all_gather(value_own, "tp", axis=0, tiled=True),
    )
    query_heads = query_all.reshape(group_rows, heads_here, HEAD)
    grad_heads = grad_all.reshape(group_rows, heads_here, HEAD)
    empty_stat = jnp.zeros((group_rows, heads_here), jnp.float32)
    empty_acc = jnp.zeros((group_rows, heads_here, HEAD), jnp.float32)
    start_state = (empty_stat, empty_acc, empty_acc, empty_acc)
    key_piece = lax.all_gather(key_group, "sp", axis=0, tiled=True)
    value_piece = lax.all_gather(value_group, "sp", axis=0, tiled=True)
    piece_rows = key_piece.shape[0]
    step_rows = block_span(piece_rows, KEY_BLOCK)

    def attend_one_block(block_index, loop_state):
        row_total, output_sum, tilted_sum, weight_sum = loop_state
        key_block = lax.dynamic_slice_in_dim(key_piece, block_index * step_rows, step_rows, 0)
        value_block = lax.dynamic_slice_in_dim(value_piece, block_index * step_rows, step_rows, 0)
        scores = (
            jnp.einsum("ihd,jd->ihj", query_heads, key_block, preferred_element_type=jnp.float32)
            * inv_root
        )
        exponent = jnp.exp(scores)
        weights = exponent.astype(jnp.bfloat16)
        prob_grad = jnp.einsum(
            "ihd,jd->ihj", grad_heads, value_block, preferred_element_type=jnp.float32
        )
        tilted = (exponent * prob_grad).astype(jnp.bfloat16)
        row_total = row_total + jnp.sum(exponent, axis=2)
        output_sum = output_sum + jnp.einsum(
            "ihj,jd->ihd", weights, value_block, preferred_element_type=jnp.float32
        )
        tilted_sum = tilted_sum + jnp.einsum(
            "ihj,jd->ihd", tilted, key_block, preferred_element_type=jnp.float32
        )
        weight_sum = weight_sum + jnp.einsum(
            "ihj,jd->ihd", weights, key_block, preferred_element_type=jnp.float32
        )
        return (row_total, output_sum, tilted_sum, weight_sum)

    row_total, output_sum, tilted_sum, weight_sum = lax.fori_loop(
        0, piece_rows // step_rows, attend_one_block, start_state
    )
    attended = (output_sum / row_total[:, :, None]).astype(jnp.bfloat16)
    delta_row = jnp.sum(attended.astype(jnp.float32) * grad_heads.astype(jnp.float32), axis=2)
    grad_query = (
        (tilted_sum - delta_row[:, :, None] * weight_sum) / row_total[:, :, None] * inv_root
    ).astype(jnp.bfloat16)
    all_total, all_delta = (
        lax.all_gather(row_total, "sp", axis=0, tiled=True),
        lax.all_gather(delta_row, "sp", axis=0, tiled=True),
    )
    empty_keys = jnp.zeros((key_group.shape[0], HEAD), jnp.float32)
    query_piece = lax.all_gather(query_all, "sp", axis=0, tiled=True)
    grad_piece = lax.all_gather(grad_all, "sp", axis=0, tiled=True)
    piece_rows = query_piece.shape[0]
    collect_step_rows = block_span(piece_rows, QUERY_BLOCK)

    def collect_one_block(block_index, loop_state):
        key_grad, value_grad = loop_state
        local_begin = block_index * collect_step_rows
        query_block = lax.dynamic_slice_in_dim(
            query_piece, local_begin, collect_step_rows, 0
        ).reshape(collect_step_rows, heads_here, HEAD)
        grad_block = lax.dynamic_slice_in_dim(
            grad_piece, local_begin, collect_step_rows, 0
        ).reshape(collect_step_rows, heads_here, HEAD)
        total_block = lax.dynamic_slice_in_dim(all_total, local_begin, collect_step_rows, 0)
        delta_block = lax.dynamic_slice_in_dim(all_delta, local_begin, collect_step_rows, 0)
        scores = (
            jnp.einsum("ihd,jd->ihj", query_block, key_group, preferred_element_type=jnp.float32)
            * inv_root
        )
        prob_rows = jnp.exp(scores) / total_block[:, :, None]
        prob_grad = jnp.einsum(
            "ihd,jd->ihj", grad_block, value_group, preferred_element_type=jnp.float32
        )
        score_grad = (prob_rows * (prob_grad - delta_block[:, :, None])).astype(jnp.bfloat16)
        key_grad = (
            key_grad
            + jnp.einsum("ihj,ihd->jd", score_grad, query_block, preferred_element_type=jnp.float32)
            * inv_root
        )
        value_grad = value_grad + jnp.einsum(
            "ihj,ihd->jd",
            prob_rows.astype(jnp.bfloat16),
            grad_block,
            preferred_element_type=jnp.float32,
        )
        return (key_grad, value_grad)

    key_grad, value_grad = lax.fori_loop(
        0, piece_rows // collect_step_rows, collect_one_block, (empty_keys, empty_keys)
    )
    key_sum, value_sum = (
        lax.psum_scatter(
            key_grad.astype(jnp.bfloat16), "tp", scatter_dimension=0, tiled=True
        ).astype(jnp.float32),
        lax.psum_scatter(
            value_grad.astype(jnp.bfloat16), "tp", scatter_dimension=0, tiled=True
        ).astype(jnp.float32),
    )
    pulled_source = right_product(key_sum.astype(jnp.bfloat16), w_key) + right_product(
        value_sum.astype(jnp.bfloat16), w_value
    )
    grad_source = norm_back(source_part, source_gain, pulled_source).astype(jnp.bfloat16)
    query_grad_rows = grad_query.reshape(group_rows, q_width)
    target_rows = group_rows // tp_count
    pulled_target = lax.psum_scatter(
        right_product(query_grad_rows, w_query).astype(jnp.bfloat16),
        "tp",
        scatter_dimension=0,
        tiled=True,
    ).astype(jnp.float32)
    target_part = lax.dynamic_slice_in_dim(target, tp_place * target_rows, target_rows, 0)
    grad_target = norm_back(target_part, target_gain, pulled_target).astype(jnp.bfloat16)
    attended_rows = attended.reshape(group_rows, q_width)
    grad_out = lax.dot_general(
        lax.all_gather(attended_rows, "sp", axis=0, tiled=True),
        cot_columns,
        (((0,), (0,)), ((), ())),
        preferred_element_type=jnp.float32,
    )
    return (grad_target, grad_source, grad_out.astype(jnp.bfloat16))


def solution(mesh):
    in_specs = (
        P("sp", None),
        P("sp", None),
        P("sp", None),
        P(),
        P(),
        P(None, "tp"),
        P(),
        P(),
        P("tp", None),
    )
    out_specs = (P(("sp", "tp"), None), P(("sp", "tp"), None), P("tp", "sp"))
    return jax.shard_map(
        on_device, mesh=mesh, in_specs=in_specs, out_specs=out_specs, check_vma=False
    )
```

profile of v0, /device:TPU:0, one launch (start us, length us, event | category | flops | bytes accessed | tf_op | source)
XLA Modules:
  0.0 221.8 jit_solution(9454115933237955824)
XLA Ops:
  7.3 2.7 %convolution_convert_fusion.2 = bf16[128,512]{1,0:T(8,128)(2,1)S(1)} fusion(bf16[128,2048]{1,0:T(8,128)(2,1)} %param.13, bf16[512,2048]{1,0:T(8,128)(2,1)} %param.19), kind=kOutput, calls=%fused_computation.33 | convolution fusion | flops 268500992 | bytes 2752512 | tf_op jit(solution)/shard_map/dot_general | solution.py:33
  10.1 12.3 %all_gather.33 = bf16[512,512]{1,0:T(8,128)(2,1)} all-gather(bf16[128,512]{1,0:T(8,128)(2,1)S(1)} %convolution_convert_fusion.2), channel_id=1, replica_groups=mesh['sp'=4,'tp'=8] {'sp'}, dimensions={0}, use_global_device_ids=true | all-gather | bytes 655360 | tf_op jit(solution)/shard_map/all_gather | solution.py:111
  24.8 14.1 %all_gather.27 = bf16[384,128]{1,0:T(8,128)(2,1)S(1)} all-gather(bf16[48,128]{1,0:T(8,128)(2,1)S(1)} %convolution_convert_fusion.5), channel_id=1, replica_groups=mesh['sp'=4,'tp'=8] {'tp'}, dimensions={0}, use_global_device_ids=true | all-gather | bytes 110592 | tf_op jit(solution)/shard_map/all_gather | solution.py:58
  38.9 9.4 %all_gather.28 = bf16[1536,128]{1,0:T(8,128)(2,1)S(1)} all-gather(bf16[384,128]{1,0:T(8,128)(2,1)S(1)} %all_gather.27), channel_id=1, replica_groups=mesh['sp'=4,'tp'=8] {'sp'}, dimensions={0}, use_global_device_ids=true | all-gather | bytes 491520 | tf_op jit(solution)/shard_map/all_gather | solution.py:66
  49.0 10.1 %all_gather.31 = bf16[512,512]{1,0:T(8,128)(2,1)} all-gather(bf16[128,512]{1,0:T(8,128)(2,1)S(1)} %convolution_convert_fusion.3), channel_id=1, replica_groups=mesh['sp'=4,'tp'=8] {'sp'}, dimensions={0}, use_global_device_ids=true | all-gather | bytes 655360 | tf_op jit(solution)/shard_map/all_gather | solution.py:110
  61.6 13.9 %all_gather.29 = bf16[384,128]{1,0:T(8,128)(2,1)S(1)} all-gather(bf16[48,128]{1,0:T(8,128)(2,1)S(1)} %convolution_convert_fusion.4), channel_id=1, replica_groups=mesh['sp'=4,'tp'=8] {'tp'}, dimensions={0}, use_global_device_ids=true | all-gather | bytes 110592 | tf_op jit(solution)/shard_map/all_gather | solution.py:59
  75.5 9.8 %all_gather.30 = bf16[1536,128]{1,0:T(8,128)(2,1)S(1)} all-gather(bf16[384,128]{1,0:T(8,128)(2,1)S(1)} %all_gather.29), channel_id=1, replica_groups=mesh['sp'=4,'tp'=8] {'sp'}, dimensions={0}, use_global_device_ids=true | all-gather | bytes 491520 | tf_op jit(solution)/shard_map/all_gather | solution.py:67
  85.3 6.8 %all_gather.32 = f32[512,4]{0,1:T(4,128)S(1)} all-gather(f32[128,4]{0,1:T(4,128)S(1)} %get-tuple-element.260), channel_id=1, replica_groups=mesh['sp'=4,'tp'=8] {'sp'}, dimensions={0}, use_global_device_ids=true | all-gather | bytes 10240 | tf_op jit(solution)/shard_map/all_gather | solution.py:106
  93.4 8.4 %all_gather.34 = f32[512,4]{0,1:T(4,128)S(1)} all-gather(f32[128,4]{0,1:T(4,128)S(1)} %get-tuple-element.262), channel_id=1, replica_groups=mesh['sp'=4,'tp'=8] {'sp'}, dimensions={0}, use_global_device_ids=true | all-gather | bytes 10240 | tf_op jit(solution)/shard_map/all_gather | solution.py:107
  101.8 16.5 %while.10 = (s32[]{:T(128)}, f32[384,128]{1,0:T(8,128)S(1)}, f32[384,128]{1,0:T(8,128)S(1)}, bf16[512,512]{1,0:T(8,128)(2,1)}, bf16[384,128]{1,0:T(8,128)(2,1)},...) while((s32[]{:T(128)}, f32[384,128]{1,0:T(8,128)S(1)}, ...), condition=%wide.region_8.0_spmd.clone, body=%wide.region_7.0_spmd.clone.sunk | while | flops 405258240 | bytes 8872134 | solution.py:148
  103.0 2.5 %exponential_divide_fusion.2 = f32[256,4,384]{2,0,1:T(8,128)} fusion(bf16[256,4,128]{0,2,1:T(8,128)(2,1)S(1)} %bitcast.95, f32[256,4]{0,1:T(4,128)S(1)} %get-tuple-element.326, bf16[384,128]{1,0:T(8,128)(2,1)} %get-tuple-element.359), kind=kOutput, calls=%fused_computation.1.clone.1 | convolution fusion | flops 101449728 | bytes 1937408 | tf_op jit(solution)/shard_map/while/body/eval_jaxpr/ihd,jd->ihj/dot_general | solution.py:127
  105.7 2.5 %fusion.92 = f32[384,128]{1,0:T(8,128)S(1)} fusion(bf16[256,4,128]{0,2,1:T(8,128)(2,1)S(1)} %bitcast.96, f32[256,4,384]{2,0,1:T(8,128)} %exponential_divide_fusion.2, bf16[256,4,128]{0,2,1:T(8,128)(2,1)S(1)} %bitcast.93, f32[256,4]{0,1:T(4,128)S(1)} %get-tuple-element.328, f32[384,128]{1,0:T(8,128)S(1)} %get-tuple-element.343, ...), kind=kOutput, calls=%fused_computation.6.clone.1 | convolution fusion | flops 202653696 | bytes 2592769 | tf_op jit(solution)/shard_map/while/body/eval_jaxpr/ihj,ihd->jd/dot_general | solution.py:137
  111.3 2.6 %exponential_divide_fusion.2 = f32[256,4,384]{2,0,1:T(8,128)} fusion(bf16[256,4,128]{0,2,1:T(8,128)(2,1)S(1)} %bitcast.95, f32[256,4]{0,1:T(4,128)S(1)} %get-tuple-element.326, bf16[384,128]{1,0:T(8,128)(2,1)} %get-tuple-element.359), kind=kOutput, calls=%fused_computation.1.clone.1 | convolution fusion | flops 101449728 | bytes 1937408 | tf_op jit(solution)/shard_map/while/body/eval_jaxpr/ihd,jd->ihj/dot_general | solution.py:127
  114.0 2.5 %fusion.92 = f32[384,128]{1,0:T(8,128)S(1)} fusion(bf16[256,4,128]{0,2,1:T(8,128)(2,1)S(1)} %bitcast.96, f32[256,4,384]{2,0,1:T(8,128)} %exponential_divide_fusion.2, bf16[256,4,128]{0,2,1:T(8,128)(2,1)S(1)} %bitcast.93, f32[256,4]{0,1:T(4,128)S(1)} %get-tuple-element.328, f32[384,128]{1,0:T(8,128)S(1)} %get-tuple-element.343, ...), kind=kOutput, calls=%fused_computation.6.clone.1 | convolution fusion | flops 202653696 | bytes 2592769 | tf_op jit(solution)/shard_map/while/body/eval_jaxpr/ihj,ihd->jd/dot_general | solution.py:137
  116.5 1.8 fusion.93
  119.0 2.0 copy.45
  121.1 4.1 %all-to-all-start = ((bf16[128,4,512]{0,2,1:T(8,128)(2,1)}), bf16[128,4,512]{0,2,1:T(8,128)(2,1)}, u32[]{:S(2)}, u32[]{:S(2)}) async-start(bf16[128,4,512]{0,2,1:T(8,128)(2,1)} %bitcast.7), calls=%async_computation.3 | async-start | bytes 1048576 | tf_op jit(solution)/shard_map/all_to_all | solution.py:49
  126.0 2.6 %convolution_multiply_fusion.2 = f32[128,4,128]{0,2,1:T(8,128)S(1)} fusion(f32[128,4,1536]{2,0,1:T(8,128)} %copy-done.1, bf16[1536,128]{1,0:T(8,128)(2,1)S(1)} %copy-done.3, f32[128,4]{0,1:T(4,128)S(1)} %get-tuple-element.262), kind=kOutput, calls=%fused_computation.28 | convolution fusion | flops 202178560 | bytes 3803136 | tf_op jit(solution)/shard_map/while/body/eval_jaxpr/ihj,jd->ihd/dot_general | solution.py:92
  128.6 3.6 %fusion.17 = bf16[128,4,128]{0,2,1:T(8,128)(2,1)} fusion(f32[128,4,128]{0,2,1:T(8,128)S(1)} %convolution_multiply_fusion.2, f32[128,4,1536]{2,0,1:T(8,128)} %copy-done.1, bf16[128,4,128]{0,2,1:T(8,128)(2,1)S(1)} %bitcast.98, bf16[1536,128]{1,0:T(8,128)(2,1)S(1)} %copy-done.5, bf16[1536,128]{1,0:T(8,128)(2,1)S(1)} %copy-done.3, ...), kind=kOutput, calls=%fused_computation.32 | convolution fusion | flops 404488192 | bytes 4458496 | tf_op jit(solution)/shard_map/while/body/eval_jaxpr/ihj,jd->ihd/dot_general | solution.py:89
  132.2 2.6 %convolution_convert_fusion = bf16[128,2048]{1,0:T(8,128)(2,1)} fusion(bf16[128,512]{0,1:T(8,128)(2,1)} %bitcast.100, bf16[2048,512]{1,0:T(8,128)(2,1)S(1)} %copy-done), kind=kOutput, calls=%fused_computation.20 | convolution fusion | flops 268697600 | bytes 2752512 | tf_op jit(solution)/shard_map/dot_general | solution.py:33
  136.4 10.5 %all_gather.35 = bf16[512,512]{0,1:T(8,128)(2,1)S(1)} all-gather(bf16[128,512]{0,1:T(8,128)(2,1)S(1)} %bitcast.99), channel_id=1, replica_groups=mesh['sp'=4,'tp'=8] {'sp'}, dimensions={0}, use_global_device_ids=true | all-gather | bytes 655360 | tf_op jit(solution)/shard_map/all_gather | solution.py:175
  146.9 2.9 %reduce-scatter.6.cloned.1.call-done = bf16[48,128]{1,0:T(8,128)(2,1)} async-done(((bf16[384,128]{1,0:T(8,128)(2,1)}), bf16[48,128]{1,0:T(8,128)(2,1)}) %reduce-scatter.6.cloned.1.call-update) | async-done | bytes 12304 | tf_op jit(solution)/shard_map/reduce_scatter | solution.py:152
  151.1 29.6 %reduce-scatter.8.cloned.1.call-done = bf16[48,128]{1,0:T(8,128)(2,1)} async-done(((bf16[384,128]{1,0:T(8,128)(2,1)}), bf16[48,128]{1,0:T(8,128)(2,1)}) %reduce-scatter.8.cloned.1.call-update) | async-done | bytes 12304 | tf_op jit(solution)/shard_map/reduce_scatter | solution.py:155
  186.4 26.2 %reduce-scatter.4.cloned.1.call-done = bf16[16,2048]{1,0:T(8,128)(2,1)} async-done(((bf16[128,2048]{1,0:T(8,128)(2,1)}), bf16[16,2048]{1,0:T(8,128)(2,1)}) %reduce-scatter.4.cloned.1.call-update) | async-done | bytes 65552 | tf_op jit(solution)/shard_map/reduce_scatter | solution.py:165
  (73 shorter events, 24.1 us)
Async XLA Ops:
  7.2 41.4 %copy-start = (bf16[2048,512]{1,0:T(8,128)(2,1)S(1)}, bf16[2048,512]{1,0:T(8,128)(2,1)}, u32[]{:S(2)}) copy-start(bf16[2048,512]{1,0:T(8,128)(2,1)} %param.16) | copy-start | bytes 6291460
  7.2 142.6 %reduce-scatter.6.cloned.1.call-start = ((), (), s32[]{:S(2)}) async-start(), calls=%async_computation.5 | async-start | bytes 110592 | tf_op jit(solution)/shard_map/reduce_scatter | solution.py:152
  7.2 16.3 %copy-start.8 = (bf16[2048,128]{1,0:T(8,128)(2,1)S(1)}, bf16[2048,128]{1,0:T(8,128)(2,1)}, u32[]{:S(2)}) copy-start(bf16[2048,128]{1,0:T(8,128)(2,1)} %param.17) | copy-start | bytes 1572868
  7.3 16.3 %copy-start.12 = (f32[2048]{0:T(1024)S(1)}, f32[2048]{0:T(1024)}, u32[]{:S(2)}) copy-start(f32[2048]{0:T(1024)} %param.15) | copy-start | bytes 24580
  10.0 38.5 %copy-start.13 = (f32[2048]{0:T(1024)S(1)}, f32[2048]{0:T(1024)}, u32[]{:S(2)}) copy-start(f32[2048]{0:T(1024)} %param.14) | copy-start | bytes 24580
  22.4 25.9 %copy-start.9 = (bf16[128,2048]{1,0:T(8,128)(2,1)S(1)}, bf16[128,2048]{1,0:T(8,128)(2,1)}, u32[]{:S(2)}) copy-start(bf16[128,2048]{1,0:T(8,128)(2,1)} %param.11) | copy-start | bytes 1572868
  23.6 36.3 %copy-start.14 = (f32[48]{0:T(128)}, f32[48]{0:T(128)S(1)}, u32[]{:S(2)}) copy-start(f32[48]{0:T(128)S(1)} %add_rsqrt_fusion) | copy-start | bytes 580
  38.9 9.6 %copy-start.11 = (bf16[384,128]{1,0:T(8,128)(2,1)}, bf16[384,128]{1,0:T(8,128)(2,1)S(1)}, u32[]{:S(2)}) copy-start(bf16[384,128]{1,0:T(8,128)(2,1)S(1)} %all_gather.27) | copy-start | bytes 294916
  48.3 10.8 %copy-start.2 = (bf16[1536,128]{1,0:T(8,128)(2,1)}, bf16[1536,128]{1,0:T(8,128)(2,1)S(1)}, u32[]{:S(2)}) copy-start(bf16[1536,128]{1,0:T(8,128)(2,1)S(1)} %all_gather.28) | copy-start | bytes 1179652
  59.1 1.0 copy-start.6
  60.2 33.3 %copy-start.1 = (f32[128,4,1536]{2,0,1:T(8,128)}, f32[128,4,1536]{2,0,1:T(8,128)S(1)}, u32[]{:S(2)}) copy-start(f32[128,4,1536]{2,0,1:T(8,128)S(1)} %get-tuple-element.261) | copy-start | bytes 9437188
  85.3 8.1 %copy-start.4 = (bf16[1536,128]{1,0:T(8,128)(2,1)}, bf16[1536,128]{1,0:T(8,128)(2,1)S(1)}, u32[]{:S(2)}) copy-start(bf16[1536,128]{1,0:T(8,128)(2,1)S(1)} %all_gather.30) | copy-start | bytes 1179652
  118.3 7.7 %copy-start.3 = (bf16[1536,128]{1,0:T(8,128)(2,1)S(1)}, bf16[1536,128]{1,0:T(8,128)(2,1)}, u32[]{:S(2)}) copy-start(bf16[1536,128]{1,0:T(8,128)(2,1)} %copy-done.2) | copy-start | bytes 1179652
  121.1 62.8 %all-to-all-start = ((bf16[128,4,512]{0,2,1:T(8,128)(2,1)}), bf16[128,4,512]{0,2,1:T(8,128)(2,1)}, u32[]{:S(2)}, u32[]{:S(2)}) async-start(bf16[128,4,512]{0,2,1:T(8,128)(2,1)} %bitcast.7), calls=%async_computation.3 | async-start | bytes 1048576 | tf_op jit(solution)/shard_map/all_to_all | solution.py:49
  125.2 55.6 %reduce-scatter.8.cloned.1.call-start = ((), (), s32[]{:S(2)}) async-start(), calls=%async_computation.6 | async-start | bytes 110592 | tf_op jit(solution)/shard_map/reduce_scatter | solution.py:155
  125.9 2.7 %copy-start.5 = (bf16[1536,128]{1,0:T(8,128)(2,1)S(1)}, bf16[1536,128]{1,0:T(8,128)(2,1)}, u32[]{:S(2)}) copy-start(bf16[1536,128]{1,0:T(8,128)(2,1)} %copy-done.4) | copy-start | bytes 1179652
  126.0 86.7 %reduce-scatter.4.cloned.1.call-start = ((), (), s32[]{:S(2)}) async-start(), calls=%async_computation.4 | async-start | bytes 589824 | tf_op jit(solution)/shard_map/reduce_scatter | solution.py:165
  132.2 4.1 %copy-start.10 = (bf16[128,4,128]{0,2,1:T(8,128)(2,1)S(1)}, bf16[128,4,128]{0,2,1:T(8,128)(2,1)}, u32[]{:S(2)}) copy-start(bf16[128,4,128]{0,2,1:T(8,128)(2,1)} %get-tuple-element.263) | copy-start | bytes 393220
  134.8 46.0 %copy-start.7 = (bf16[2048,128]{1,0:T(8,128)(2,1)S(1)}, bf16[2048,128]{1,0:T(8,128)(2,1)}, u32[]{:S(2)}) copy-start(bf16[2048,128]{1,0:T(8,128)(2,1)} %param.18) | copy-start | bytes 1572868
  182.1 30.5 %copy-start.15 = (f32[16]{0:T(128)S(1)}, f32[16]{0:T(128)}, u32[]{:S(2)}) copy-start(f32[16]{0:T(128)} %add_rsqrt_fusion.2) | copy-start | bytes 196
Sparse Core Ops, SparseCore 0:
  119.1 30.5 reduce-scatter.5
  152.0 28.7 reduce-scatter.7
  183.0 29.5 reduce-scatter.3
where the time goes:
time: 223 us; the launch traced here: 222 us
  blocking collectives  95.2 us (43%)
  waiting for transfers between devices  58.9 us (26%)
  matrix products  34.2 us (15%)
  between operations  14 us (6%)
  other arithmetic  8.6 us (4%)
  local copies, waits for them, and re-layouts  6.51 us (3%)
  starting transfers between devices  4.25 us (2%)
    reduce_scatter x1, waiting for transfers between devices, on_device(): lax.psum_scatter(value_grad.astype(jnp.bfloat16), 'tp', scatter_dimension...  29.6 us
    reduce_scatter x1, waiting for transfers between devices, on_device(): lax.psum_scatter(right_product(query_grad_rows, w_query).astype(jnp.bfloa...  26.2 us
    all_gather x1, blocking collectives, on_device(): lax.all_gather(key_own, 'tp', axis=0, tiled=True)  14.1 us
    all_gather x1, blocking collectives, on_device(): lax.all_gather(value_own, 'tp', axis=0, tiled=True)  13.9 us
    all_gather x1, blocking collectives, on_device(): grad_piece = lax.all_gather(grad_all, 'sp', axis=0, tiled=True)  12.3 us
    all_gather x1, blocking collectives, on_device(): lax.all_gather(attended_rows, 'sp', axis=0, tiled=True)  10.5 us
    all_gather x1, blocking collectives, on_device(): query_piece = lax.all_gather(query_all, 'sp', axis=0, tiled=True)  10.1 us
    all_gather x1, blocking collectives, on_device(): value_piece = lax.all_gather(value_group, 'sp', axis=0, tiled=True)  9.79 us
  transfers between devices with their start and end apart: 4, of which 3 were waited for; matrix products, arithmetic and copies ran while one was open for 9% of the time, Pallas kernels for 0%

commit v1 on v0

--- a/solution.py
+++ b/solution.py
@@ -107,8 +107,11 @@
         lax.all_gather(delta_row, "sp", axis=0, tiled=True),
     )
     empty_keys = jnp.zeros((key_group.shape[0], HEAD), jnp.float32)
-    query_piece = lax.all_gather(query_all, "sp", axis=0, tiled=True)
-    grad_piece = lax.all_gather(grad_all, "sp", axis=0, tiled=True)
+    query_piece, grad_piece = jnp.split(
+        lax.all_gather(jnp.concatenate([query_all, grad_all], axis=1), "sp", axis=0, tiled=True),
+        [query_all.shape[1]],
+        axis=1,
+    )
     piece_rows = query_piece.shape[0]
     collect_step_rows = block_span(piece_rows, QUERY_BLOCK)
 

time: 223 us -> 210 us (0.942)
  blocking collectives: 95.2 us -> 77.7 us
  local copies, waits for them, and re-layouts: 6.51 us -> 12 us
  matrix products: 34.2 us -> 31.5 us
    reduce_scatter x1, waiting for transfers between devices: 26.2 us -> 0.01 us  [on_device(): lax.psum_scatter(right_product(query_grad_rows, w_query).astype(jnp.bfloa...]
    reduce_scatter x1, waiting for transfers between devices: 2.91 us -> 28.3 us  [on_device(): lax.psum_scatter(key_grad.astype(jnp.bfloat16), 'tp', scatter_dimension=0...]
    all_gather x2 -> x0, blocking collectives: 22.4 us -> none  [the longest x1 12.3 us: on_device(): grad_piece = lax.all_gather(grad_all, 'sp', axis=0, tiled=True)]
    all_gather x1, blocking collectives: 6.79 us -> 10.6 us  [on_device(): lax.all_gather(row_total, 'sp', axis=0, tiled=True)]
    split x0 -> x1, local copies, waits for them, and re-layouts: none -> 2.23 us  [on_device(): jnp.split(lax.all_gather(jnp.concatenate([query_all, grad_all], axis=1),...]
  transfers between devices with their start and end apart: 4 -> 5, of which waited for: 3 -> 2; matrix products, arithmetic and copies ran while one was open for 9% -> 6% of each run, Pallas kernels for 0% -> 0%
where the time goes in v1:
time: 210 us; the launch traced here: 209 us
  blocking collectives  77.7 us (37%)
  waiting for transfers between devices  58.1 us (28%)
  matrix products  31.5 us (15%)
  between operations  15.5 us (7%)
  local copies, waits for them, and re-layouts  12 us (6%)
  other arithmetic  9.95 us (5%)
  starting transfers between devices  4.31 us (2%)
    reduce_scatter x1, waiting for transfers between devices, on_device(): lax.psum_scatter(value_grad.astype(jnp.bfloat16), 'tp', scatter_dimension...  29.7 us
    reduce_scatter x1, waiting for transfers between devices, on_device(): lax.psum_scatter(key_grad.astype(jnp.bfloat16), 'tp', scatter_dimension=0...  28.3 us
    all_gather x1, blocking collectives, on_device(): lax.all_gather(key_own, 'tp', axis=0, tiled=True)  15.6 us
    all_gather x1, blocking collectives, on_device(): lax.all_gather(value_own, 'tp', axis=0, tiled=True)  13.9 us
    all_gather x1, blocking collectives, on_device(): lax.all_gather(attended_rows, 'sp', axis=0, tiled=True)  10.7 us
    all_gather x1, blocking collectives, on_device(): lax.all_gather(row_total, 'sp', axis=0, tiled=True)  10.6 us
    all_gather x1, blocking collectives, on_device(): key_piece = lax.all_gather(key_group, 'sp', axis=0, tiled=True)  9.5 us
    all_gather x1, blocking collectives, on_device(): value_piece = lax.all_gather(value_group, 'sp', axis=0, tiled=True)  9.48 us
  transfers between devices with their start and end apart: 5, of which 2 were waited for; matrix products, arithmetic and copies ran while one was open for 6% of the time, Pallas kernels for 0%

profile of v1, /device:TPU:0, one launch (start us, length us, event | category | flops | bytes accessed | tf_op | source)
XLA Modules:
  0.0 209.2 jit_solution(1986425549091934133)
XLA Ops:
  10.8 15.6 %all_gather.24 = bf16[384,128]{1,0:T(8,128)(2,1)S(1)} all-gather(bf16[48,128]{1,0:T(8,128)(2,1)S(1)} %convolution_convert_fusion.5), channel_id=1, replica_groups=mesh['sp'=4,'tp'=8] {'tp'}, dimensions={0}, use_global_device_ids=true | all-gather | bytes 110592 | tf_op jit(solution)/shard_map/all_gather | solution.py:58
  27.0 9.5 %all_gather.25 = bf16[1536,128]{1,0:T(8,128)(2,1)S(1)} all-gather(bf16[384,128]{1,0:T(8,128)(2,1)S(1)} %all_gather.24), channel_id=1, replica_groups=mesh['sp'=4,'tp'=8] {'sp'}, dimensions={0}, use_global_device_ids=true | all-gather | bytes 491520 | tf_op jit(solution)/shard_map/all_gather | solution.py:66
  37.3 3.1 %convolution_convert_fusion.2 = bf16[128,512]{1,0:T(8,128)(2,1)} fusion(bf16[128,2048]{1,0:T(8,128)(2,1)S(1)} %copy-done.4, bf16[512,2048]{1,0:T(8,128)(2,1)} %param.19), kind=kOutput, calls=%fused_computation.33 | convolution fusion | flops 268500992 | bytes 2752512 | tf_op jit(solution)/shard_map/dot_general | solution.py:33
  42.6 13.9 %all_gather.26 = bf16[384,128]{1,0:T(8,128)(2,1)S(1)} all-gather(bf16[48,128]{1,0:T(8,128)(2,1)S(1)} %convolution_convert_fusion.4), channel_id=1, replica_groups=mesh['sp'=4,'tp'=8] {'tp'}, dimensions={0}, use_global_device_ids=true | all-gather | bytes 110592 | tf_op jit(solution)/shard_map/all_gather | solution.py:59
  56.6 9.5 %all_gather.27 = bf16[1536,128]{1,0:T(8,128)(2,1)S(1)} all-gather(bf16[384,128]{1,0:T(8,128)(2,1)S(1)} %all_gather.26), channel_id=1, replica_groups=mesh['sp'=4,'tp'=8] {'sp'}, dimensions={0}, use_global_device_ids=true | all-gather | bytes 491520 | tf_op jit(solution)/shard_map/all_gather | solution.py:67
  71.3 2.9 %fusion.17 = bf16[128,4,128]{0,2,1:T(8,128)(2,1)S(1)} fusion(f32[128,4,128]{0,2,1:T(8,128)} %convolution_multiply_fusion.2, f32[128,4,1536]{2,0,1:T(8,128)} %copy-done.1, bf16[128,4,128]{0,2,1:T(8,128)(2,1)S(1)} %bitcast.98, bf16[1536,128]{1,0:T(8,128)(2,1)S(1)} %all_gather.27, bf16[1536,128]{1,0:T(8,128)(2,1)S(1)} %all_gather.25, ...), kind=kOutput, calls=%fused_computation.32 | convolution fusion | flops 404488192 | bytes 4458496 | tf_op jit(solution)/shard_map/while/body/eval_jaxpr/ihj,jd->ihd/dot_general | solution.py:89
  74.3 1.6 convolution_convert_fusion
  77.8 4.1 %all-to-all-start = ((bf16[128,4,512]{0,2,1:T(8,128)(2,1)}), bf16[128,4,512]{0,2,1:T(8,128)(2,1)}, u32[]{:S(2)}, u32[]{:S(2)}) async-start(bf16[128,4,512]{0,2,1:T(8,128)(2,1)} %bitcast.7), calls=%async_computation.3 | async-start | bytes 1048576 | tf_op jit(solution)/shard_map/all_to_all | solution.py:49
  82.0 10.6 %all_gather.29 = f32[512,4]{0,1:T(4,128)S(1)} all-gather(f32[128,4]{0,1:T(4,128)S(1)} %get-tuple-element.262), channel_id=1, replica_groups=mesh['sp'=4,'tp'=8] {'sp'}, dimensions={0}, use_global_device_ids=true | all-gather | bytes 10240 | tf_op jit(solution)/shard_map/all_gather | solution.py:106
  92.7 7.8 %all_gather.30 = f32[512,4]{0,1:T(4,128)} all-gather(f32[128,4]{0,1:T(4,128)S(1)} %get-tuple-element.264), channel_id=1, replica_groups=mesh['sp'=4,'tp'=8] {'sp'}, dimensions={0}, use_global_device_ids=true | all-gather | bytes 10240 | tf_op jit(solution)/shard_map/all_gather | solution.py:107
  101.4 10.7 %all_gather.31 = bf16[512,512]{0,1:T(8,128)(2,1)S(1)} all-gather(bf16[128,512]{0,1:T(8,128)(2,1)S(1)} %bitcast.99), channel_id=1, replica_groups=mesh['sp'=4,'tp'=8] {'sp'}, dimensions={0}, use_global_device_ids=true | all-gather | bytes 655360 | tf_op jit(solution)/shard_map/all_gather | solution.py:178
  112.2 2.1 copy.46
  114.2 2.3 %convolution_convert_fusion.1 = bf16[512,512]{1,0:T(8,128)(2,1)} fusion(bf16[512,512]{0,1:T(8,128)(2,1)S(1)} %all_gather.31, bf16[512,512]{1,0:T(8,128)(2,1)} %bitcast.97), kind=kOutput, calls=%fused_computation.26 | convolution fusion | flops 268697600 | bytes 1572864 | tf_op jit(solution)/shard_map/dot_general | solution.py:177
  118.2 2.2 %fusion.55 = (bf16[512,512]{1,0:T(8,128)(2,1)}, bf16[512,512]{1,0:T(8,128)(2,1)}) fusion(bf16[512,1024]{1,0:T(8,128)(2,1)} %all-gather.2.cloned.1.call-done), kind=kLoop, calls=%fused_computation.82 | loop fusion | bytes 2097152 | tf_op jit(solution)/shard_map/split | solution.py:110
  120.5 16.1 %while.10 = (s32[]{:T(128)}, f32[384,128]{1,0:T(8,128)S(1)}, f32[384,128]{1,0:T(8,128)S(1)}, bf16[512,512]{1,0:T(8,128)(2,1)}, bf16[384,128]{1,0:T(8,128)(2,1)S(...) while((s32[]{:T(128)}, f32[384,128]{1,0:T(8,128)S(1)}, ...), condition=%wide.region_8.0_spmd.clone, body=%wide.region_7.0_spmd.clone.sunk | while | flops 405258240 | bytes 8872134 | solution.py:151
  122.4 1.7 exponential_divide_fusion.2
  124.2 2.5 %fusion.93 = f32[384,128]{1,0:T(8,128)S(1)} fusion(bf16[256,4,128]{0,2,1:T(8,128)(2,1)S(1)} %bitcast.96, f32[256,4,384]{2,0,1:T(8,128)} %exponential_divide_fusion.2, bf16[256,4,128]{0,2,1:T(8,128)(2,1)S(1)} %bitcast.93, f32[256,4]{0,1:T(4,128)S(1)} %get-tuple-element.330, f32[384,128]{1,0:T(8,128)S(1)} %get-tuple-element.345, ...), kind=kOutput, calls=%fused_computation.6.clone.1 | convolution fusion | flops 202653696 | bytes 2592769 | tf_op jit(solution)/shard_map/while/body/eval_jaxpr/ihj,ihd->jd/dot_general | solution.py:140
  126.7 1.8 fusion.94
  130.4 1.7 exponential_divide_fusion.2
  132.2 2.5 %fusion.93 = f32[384,128]{1,0:T(8,128)S(1)} fusion(bf16[256,4,128]{0,2,1:T(8,128)(2,1)S(1)} %bitcast.96, f32[256,4,384]{2,0,1:T(8,128)} %exponential_divide_fusion.2, bf16[256,4,128]{0,2,1:T(8,128)(2,1)S(1)} %bitcast.93, f32[256,4]{0,1:T(4,128)S(1)} %get-tuple-element.330, f32[384,128]{1,0:T(8,128)S(1)} %get-tuple-element.345, ...), kind=kOutput, calls=%fused_computation.6.clone.1 | convolution fusion | flops 202653696 | bytes 2592769 | tf_op jit(solution)/shard_map/while/body/eval_jaxpr/ihj,ihd->jd/dot_general | solution.py:140
  134.7 1.8 fusion.94
  139.6 28.3 %reduce-scatter.6.cloned.1.call-done = bf16[48,128]{1,0:T(8,128)(2,1)} async-done(((bf16[384,128]{1,0:T(8,128)(2,1)}), bf16[48,128]{1,0:T(8,128)(2,1)}) %reduce-scatter.6.cloned.1.call-update) | async-done | bytes 12304 | tf_op jit(solution)/shard_map/reduce_scatter | solution.py:155
  169.2 29.7 %reduce-scatter.8.cloned.1.call-done = bf16[48,128]{1,0:T(8,128)(2,1)} async-done(((bf16[384,128]{1,0:T(8,128)(2,1)}), bf16[48,128]{1,0:T(8,128)(2,1)}) %reduce-scatter.8.cloned.1.call-update) | async-done | bytes 12304 | tf_op jit(solution)/shard_map/reduce_scatter | solution.py:158
  200.3 1.7 fusion.34
  (80 shorter events, 25.8 us)
Async XLA Ops:
  8.0 58.1 %copy-start = (bf16[2048,512]{1,0:T(8,128)(2,1)S(1)}, bf16[2048,512]{1,0:T(8,128)(2,1)}, u32[]{:S(2)}) copy-start(bf16[2048,512]{1,0:T(8,128)(2,1)} %param.16) | copy-start | bytes 6291460
  8.0 28.5 %copy-start.7 = (bf16[128,2048]{1,0:T(8,128)(2,1)S(1)}, bf16[128,2048]{1,0:T(8,128)(2,1)}, u32[]{:S(2)}) copy-start(bf16[128,2048]{1,0:T(8,128)(2,1)} %param.11) | copy-start | bytes 1572868
  8.0 29.3 %copy-start.4 = (bf16[128,2048]{1,0:T(8,128)(2,1)S(1)}, bf16[128,2048]{1,0:T(8,128)(2,1)}, u32[]{:S(2)}) copy-start(bf16[128,2048]{1,0:T(8,128)(2,1)} %param.13) | copy-start | bytes 1572868
  8.0 108.5 %reduce-scatter.4.cloned.1.call-start = ((), (), s32[]{:S(2)}) async-start(), calls=%async_computation.4 | async-start | bytes 589824 | tf_op jit(solution)/shard_map/reduce_scatter | solution.py:168
  9.3 17.1 %copy-start.15 = (f32[48]{0:T(128)}, f32[48]{0:T(128)S(1)}, u32[]{:S(2)}) copy-start(f32[48]{0:T(128)S(1)} %add_rsqrt_fusion) | copy-start | bytes 580
  26.4 0.6 copy-start.8
  36.7 4.7 %copy-start.2 = (bf16[2048,128]{1,0:T(8,128)(2,1)S(1)}, bf16[2048,128]{1,0:T(8,128)(2,1)}, u32[]{:S(2)}) copy-start(bf16[2048,128]{1,0:T(8,128)(2,1)} %param.18) | copy-start | bytes 1572868
  36.7 4.7 %copy-start.11 = (f32[2048]{0:T(1024)S(1)}, f32[2048]{0:T(1024)}, u32[]{:S(2)}) copy-start(f32[2048]{0:T(1024)} %param.15) | copy-start | bytes 24580
  37.3 28.8 %copy-start.13 = (f32[2048]{0:T(1024)S(1)}, f32[2048]{0:T(1024)}, u32[]{:S(2)}) copy-start(f32[2048]{0:T(1024)} %param.14) | copy-start | bytes 24580
  40.4 25.7 %copy-start.17 = (f32[128]{0:T(128)S(1)}, f32[128]{0:T(128)}, u32[]{:S(2)}) copy-start(f32[128]{0:T(128)} %add_rsqrt_fusion.1) | copy-start | bytes 1540
  68.3 1.6 copy-start.1
  74.3 1.7 copy-start.6
  74.3 2.5 %copy-start.5 = (bf16[128,2048]{1,0:T(8,128)(2,1)S(1)}, bf16[128,2048]{1,0:T(8,128)(2,1)}, u32[]{:S(2)}) copy-start(bf16[128,2048]{1,0:T(8,128)(2,1)} %param.13) | copy-start | bytes 1572868
  76.0 42.2 %all-gather.2.cloned.1.call-start = ((), (), s32[]{:S(2)}) async-start(), calls=%async_computation.5 | async-start | bytes 1310720 | tf_op jit(solution)/shard_map/all_gather | solution.py:111
  77.8 34.4 %all-to-all-start = ((bf16[128,4,512]{0,2,1:T(8,128)(2,1)}), bf16[128,4,512]{0,2,1:T(8,128)(2,1)}, u32[]{:S(2)}, u32[]{:S(2)}) async-start(bf16[128,4,512]{0,2,1:T(8,128)(2,1)} %bitcast.7), calls=%async_computation.3 | async-start | bytes 1048576 | tf_op jit(solution)/shard_map/all_to_all | solution.py:49
  82.0 85.9 %reduce-scatter.6.cloned.1.call-start = ((), (), s32[]{:S(2)}) async-start(), calls=%async_computation.6 | async-start | bytes 110592 | tf_op jit(solution)/shard_map/reduce_scatter | solution.py:155
  101.4 15.1 %copy-start.14 = (f32[2048]{0:T(1024)S(1)}, f32[2048]{0:T(1024)}, u32[]{:S(2)}) copy-start(f32[2048]{0:T(1024)} %param.14) | copy-start | bytes 24580
  114.2 6.2 %copy-start.9 = (bf16[384,128]{1,0:T(8,128)(2,1)S(1)}, bf16[384,128]{1,0:T(8,128)(2,1)}, u32[]{:S(2)}) copy-start(bf16[384,128]{1,0:T(8,128)(2,1)} %copy-done.8) | copy-start | bytes 294916
  120.5 16.9 %copy-start.10 = (bf16[16,2048]{1,0:T(8,128)(2,1)S(1)}, bf16[16,2048]{1,0:T(8,128)(2,1)}, u32[]{:S(2)}) copy-start(bf16[16,2048]{1,0:T(8,128)(2,1)} %reduce-scatter.4.cloned.1.call-done) | copy-start | bytes 196612
  136.6 62.4 %copy-start.3 = (bf16[2048,128]{1,0:T(8,128)(2,1)S(1)}, bf16[2048,128]{1,0:T(8,128)(2,1)}, u32[]{:S(2)}) copy-start(bf16[2048,128]{1,0:T(8,128)(2,1)} %param.18) | copy-start | bytes 1572868
  136.6 62.4 %copy-start.12 = (f32[2048]{0:T(1024)S(1)}, f32[2048]{0:T(1024)}, u32[]{:S(2)}) copy-start(f32[2048]{0:T(1024)} %param.15) | copy-start | bytes 24580
  136.6 62.4 %copy-start.16 = (f32[48]{0:T(128)S(1)}, f32[48]{0:T(128)}, u32[]{:S(2)}) copy-start(f32[48]{0:T(128)} %copy-done.15) | copy-start | bytes 580
  137.3 61.7 %reduce-scatter.8.cloned.1.call-start = ((), (), s32[]{:S(2)}) async-start(), calls=%async_computation.7 | async-start | bytes 110592 | tf_op jit(solution)/shard_map/reduce_scatter | solution.py:158
Sparse Core Ops, SparseCore 0:
  76.1 31.3 reduce-scatter.3
  137.4 30.4 reduce-scatter.5
  170.1 28.7 reduce-scatter.7
Sparse Core Ops, SparseCore 1:
  78.3 28.0 all-gather.1
